TPU v7x, 32 devices: a whole 2x2x4 slice. The times are simulated.
32 devices in a mesh: sp: 8 (over z, x), tp: 4 (over y, core).
Axes of the slice: x: 2, y: 2, z: 4, core: 2. Of those that a mesh axis runs over, the one named last changes fastest.
Arguments:
- residual: bfloat16 [1024, 2048], P('sp'), may hold values from -6 to 6
- queries: bfloat16 [1024, 2048], P('sp', 'tp'), may hold values from -6 to 6
- keys: bfloat16 [1024, 2048], P('sp', 'tp'), may hold values from -6 to 6
- values: bfloat16 [1024, 2048], P('sp', 'tp'), may hold values from -24 to 24
- stick_bias: bfloat16 [32, 1024], P('tp', 'sp'), may hold values from 2 to 13
- query_gain: float32 [64], replicated, may hold values from 0.1 to 1.9
- key_gain: float32 [64], replicated, may hold values from 0.1 to 1.9
- out_weight: bfloat16 [2048, 2048], P('tp'), may hold values from -0.25 to 0.25
- norm_gain: float32 [2048], replicated, may hold values from 0.1 to 1.9
- route_ids: int32 [1024, 2], P('sp'), may hold values from 0 to 7, all different within a row; in each aligned block of 128 rows (0 to 127, 128 to 255, ...) at most 40 rows name the same one
- route_weights: float32 [1024, 2], P('sp'), may hold values from 0.1 to 1
- gate_weight: bfloat16 [8, 2048, 2048], P('sp', None, 'tp'), may hold values from -3 to 3
- up_weight: bfloat16 [8, 2048, 2048], P('sp', None, 'tp'), may hold values from -3 to 3
- down_weight: bfloat16 [8, 2048, 2048], P('sp', 'tp'), may hold values from -0.125 to 0.125
Outputs:
- layer_out: bfloat16 [1024, 2048], P('sp', 'tp')
Inputs may be any that keep to these rules, and one draw needn't show every extreme that they name: `route_ids`: each row names 2 different experts. In every aligned block of 128 rows at most 40 rows name one expert, and in every draw some expert is named by exactly 40 rows of some block.
All inputs are finite; a program needn't handle non-finite values.
Results may differ from a plain program's by a relative error of at most 0.028.
Values may be sent and summed in bfloat16 or wider, within the bound.
A program may use at most 64 MiB of HBM per device.

v0:
```python
import math

import jax
import jax.numpy as jnp
from jax import lax
from jax.sharding import PartitionSpec as P

epsilon = 1e-06
clamp_limit = 7.0
swish_scale = 1.702


def head_normalize(packed, gain):
    values_f = packed.astype(jnp.float32).reshape(packed.shape[0], -1, gain.shape[0])
    scaled = (
        values_f * lax.rsqrt(jnp.mean(values_f * values_f, axis=-1, keepdims=True) + epsilon) * gain
    )
    return scaled.astype(jnp.bfloat16)


def activate(gate_pre, up_pre):
    gate_top = jnp.minimum(gate_pre, clamp_limit)
    up_clip = jnp.clip(up_pre, -clamp_limit, clamp_limit)
    return (up_clip + 1.0) * (gate_top * jax.nn.sigmoid(swish_scale * gate_top))


def slot_table(picked, expert_count, capacity):
    flat_ids = picked.reshape(-1)
    one_hot = (flat_ids[:, None] == jnp.arange(expert_count, dtype=jnp.int32)[None, :]).astype(
        jnp.int32
    )
    before = jnp.sum((jnp.cumsum(one_hot, axis=0) - one_hot) * one_hot, axis=1)
    return flat_ids * capacity + before


def key_block(state_pair, queries_n, keys_block, values_block, bias_block, first_key, query_pos):
    summed, log_carry = state_pair
    key_count = bias_block.shape[1]
    head_total = bias_block.shape[0]
    keys_heads = keys_block.reshape(key_count, head_total, -1)
    values_heads = values_block.reshape(key_count, head_total, -1)
    head_dim = keys_heads.shape[2]
    scores = jnp.einsum(
        "qhd,khd->hqk", queries_n, keys_heads, preferred_element_type=jnp.float32
    ) * head_dim ** (-0.5)
    scores = scores - bias_block.astype(jnp.float32)[:, None, :]
    key_pos = first_key + jnp.arange(key_count, dtype=jnp.int32)
    causal = ((key_pos[None, :] < query_pos[:, None]) & (key_pos[None, :] >= 0))[None]
    log_stay = jnp.where(causal, jax.nn.log_sigmoid(-scores), 0.0)
    later_sum = lax.cumsum(log_stay, axis=2, reverse=True) - log_stay
    weight = jnp.where(
        causal, jnp.exp(jax.nn.log_sigmoid(scores) + later_sum + log_carry[:, :, None]), 0.0
    )
    summed = summed + jnp.einsum(
        "hqk,khd->qhd",
        weight.astype(jnp.bfloat16),
        values_heads,
        preferred_element_type=jnp.float32,
    )
    return (summed, log_carry + jnp.sum(log_stay, axis=2))


def per_device(
    residual,
    queries,
    keys,
    values,
    stick_bias,
    query_gain,
    key_gain,
    out_weight,
    norm_gain,
    route_ids,
    route_weights,
    gate_weight,
    up_weight,
    down_weight,
):
    tok_rows = queries.shape[0]
    width_sp = lax.axis_size("sp")
    offset = lax.axis_index("sp") * tok_rows
    query_pos = offset + jnp.arange(tok_rows, dtype=jnp.int32)
    queries_n = head_normalize(queries, query_gain)
    keys_n = head_normalize(keys, key_gain).reshape(tok_rows, -1)
    head_total = stick_bias.shape[0]
    head_dim = query_gain.shape[0]
    state_pair = (
        jnp.zeros((tok_rows, head_total, head_dim), jnp.float32),
        jnp.zeros((head_total, tok_rows), jnp.float32),
    )
    all_keys, all_values, all_bias = (
        lax.all_gather(keys_n, "sp", axis=0, tiled=True),
        lax.all_gather(values, "sp", axis=0, tiled=True),
        lax.all_gather(stick_bias, "sp", axis=1, tiled=True),
    )
    key_total = all_keys.shape[0]
    block_len = math.gcd(key_total, 512)
    block_total = key_total // block_len

    def sweep_block(block_step, running):
        first_key = (block_total - 1 - block_step) * block_len
        return key_block(
            running,
            queries_n,
            lax.dynamic_slice_in_dim(all_keys, first_key, block_len, 0),
            lax.dynamic_slice_in_dim(all_values, first_key, block_len, 0),
            lax.dynamic_slice_in_dim(all_bias, first_key, block_len, 1),
            first_key,
            query_pos,
        )

    state_pair = lax.fori_loop(0, block_total, sweep_block, state_pair)
    attended = state_pair[0].reshape(tok_rows, head_total * head_dim).astype(jnp.bfloat16)
    partial_value = jnp.dot(attended, out_weight, preferred_element_type=jnp.float32)
    model_width = residual.shape[1]
    expert_count = width_sp * gate_weight.shape[0]
    pick_count = route_ids.shape[1]
    capacity = (5 * tok_rows * pick_count + 4 * expert_count - 1) // (4 * expert_count)
    slot_index = slot_table(route_ids, expert_count, capacity)
    assigned = slot_index.shape[0]
    source = (
        jnp.zeros((expert_count * capacity,), jnp.int32)
        .at[slot_index]
        .set(jnp.arange(assigned, dtype=jnp.int32) // pick_count)
    )
    filled = (
        jnp.zeros((expert_count * capacity,), jnp.bfloat16)
        .at[slot_index]
        .set(jnp.ones((assigned,), jnp.bfloat16))
    )
    gate_local = gate_weight[0]
    up_local = up_weight[0]
    down_local = down_weight[0]
    mixed_share = lax.psum_scatter(
        partial_value.astype(jnp.bfloat16), "tp", scatter_dimension=1, tiled=True
    ).astype(jnp.float32)
    own_width = mixed_share.shape[1]
    col_start = lax.axis_index("tp") * own_width
    own_res = lax.dynamic_slice_in_dim(residual, col_start, own_width, 1).astype(jnp.float32)
    own_cols = (own_res + mixed_share).astype(jnp.bfloat16).astype(jnp.float32)
    square_total = lax.psum(jnp.sum(own_cols * own_cols, axis=1), "tp")
    gain_cols = lax.dynamic_slice_in_dim(norm_gain, col_start, own_width, 0)
    normed_share = (
        own_cols * lax.rsqrt(square_total / model_width + epsilon)[:, None] * gain_cols
    ).astype(jnp.bfloat16)
    outgoing = (normed_share[source] * filled[:, None]).reshape(expert_count, capacity, -1)
    piece = lax.all_gather(
        lax.all_to_all(outgoing, "sp", split_axis=0, concat_axis=0, tiled=True),
        "tp",
        axis=2,
        tiled=True,
    )
    gate_pre = jnp.einsum("scd,df->scf", piece, gate_local, preferred_element_type=jnp.float32)
    up_pre = jnp.einsum("scd,df->scf", piece, up_local, preferred_element_type=jnp.float32)
    hidden = activate(gate_pre, up_pre).astype(jnp.bfloat16)
    share = jnp.einsum("scf,fd->scd", hidden, down_local, preferred_element_type=jnp.float32)
    returned = lax.psum_scatter(share.astype(jnp.bfloat16), "tp", scatter_dimension=2, tiled=True)
    arrived = lax.all_to_all(returned, "sp", split_axis=0, concat_axis=0, tiled=True)
    columns = arrived.shape[2]
    taken_rows = arrived.reshape(expert_count * capacity, columns)[slot_index]
    taken_rows = taken_rows.astype(jnp.float32).reshape(tok_rows, pick_count, columns)
    routed = jnp.sum(taken_rows * route_weights[:, :, None], axis=1)
    return (own_cols + routed).astype(jnp.bfloat16)


def solution(mesh):
    placed = (
        P("sp", None),
        P("sp", "tp"),
        P("sp", "tp"),
        P("sp", "tp"),
        P("tp", "sp"),
        P(),
        P(),
        P("tp", None),
        P(),
        P("sp", None),
        P("sp", None),
        P("sp", None, "tp"),
        P("sp", None, "tp"),
        P("sp", "tp", None),
    )
    return jax.shard_map(
        per_device, mesh=mesh, in_specs=placed, out_specs=P("sp", "tp"), check_vma=False
    )
```

profile of v0, /device:TPU:0, one launch (start us, length us, event | category | flops | bytes accessed | tf_op | source)
XLA Modules:
  0.0 249.5 jit_solution(2540238676448930279)
XLA Ops:
  6.5 1.2 copy.26
  9.4 1.7 copy.25
  11.1 1.0 copy.27
  13.7 28.2 %all_gather.14 = bf16[8,1024]{1,0:T(8,128)(2,1)S(1)} all-gather(bf16[8,128]{1,0:T(8,128)(2,1)} %param.20), channel_id=1, replica_groups=mesh['sp'=8,'tp'=4] {'sp'}, dimensions={1}, use_global_device_ids=true | all-gather | bytes 18432 | tf_op jit(solution)/shard_map/all_gather | solution.py:94
  42.7 8.9 %all-gather.6.cloned.1.call-done = bf16[1024,512]{0,1:T(8,128)(2,1)} async-done(((bf16[128,512]{0,1:T(8,128)(2,1)}), bf16[1024,512]{0,1:T(8,128)(2,1)}) %all-gather.6.cloned.1.call-update) | async-done | bytes 1048592 | tf_op jit(solution)/shard_map/all_gather | solution.py:92
  51.6 40.3 %all-gather.4.cloned.1.call-done = bf16[1024,512]{0,1:T(8,128)(2,1)} async-done(((bf16[128,512]{0,1:T(8,128)(2,1)}), bf16[1024,512]{0,1:T(8,128)(2,1)}) %all-gather.4.cloned.1.call-update) | async-done | bytes 1048592 | tf_op jit(solution)/shard_map/all_gather | solution.py:93
  91.9 33.3 %while.16 = (s32[]{:T(128)}, f32[128,8,64]{0,2,1:T(8,128)S(1)}, f32[8,128]{1,0:T(8,128)S(1)}, bf16[1024,512]{0,1:T(8,128)(2,1)}, bf16[1024,512]{0,1:T(8,128)(2,1...) while((s32[]{:T(128)}, f32[128,8,64]{0,2,1:T(8,128)S(1)}, ...), condition=%wide.region_6.7_spmd.clone, body=%wide.region_2.6_spmd.clone.sunk | while | flops 219436672 | bytes 27240652 | solution.py:112
  91.9 1.3 constant_dynamic-slice_fusion.3
  93.4 3.0 %fusion.93 = (f32[8,128]{1,0:T(8,128)S(1)}, f32[8,128,512]{1,2,0:T(8,128)S(1)}, f32[8,512,128]{2,1,0:T(8,128)}) fusion(f32[8,512]{1,0:T(8,128)S(1)} %dynamic-slice_convert_fusion.2, pred[128,512]{0,1:T(8,128)(4,1)S(1)} %compare_and_fusion.2, bf16[512,8,64]{0,2,1:T(8,128)(2,1)S(1)} %bitcast.116, bf16[128,8,64]{0,2,1:T(8,128)(2,1)S(1)} %get-tuple-element.292), kind=kOutput, calls=%fused_computation.39.clone.1 | convolution fusion | flops 72875008 | bytes 4935680 | tf_op jit(solution)/shard_map/while/body/eval_jaxpr/qhd,khd->hqk/dot_general | solution.py:43
  96.4 5.0 %fusion.94 = f32[8,128,4,128]{1,0,3,2:T(8,128)S(1)} fusion(f32[8,128,4,128]{1,3,2,0:T(8,128)S(1)} %bitcast.114), kind=kOutput, calls=%fused_computation.23.clone.1 | output fusion | flops 66584576 | bytes 4194304 | tf_op jit(solution)/shard_map/reduce-window.6
  101.6 1.7 copy.38
  103.3 4.8 %fusion.97 = bf16[8,128,512]{1,2,0:T(8,128)(2,1)S(1)} fusion(f32[8,128,4,128]{1,3,2,0:T(8,128)} %copy.38, f32[8,512,128]{2,1,0:T(8,128)} %get-tuple-element.259, f32[8,128]{1,0:T(8,128)S(1)} %get-tuple-element.261, f32[8,512]{1,0:T(8,128)S(1)} %dynamic-slice_convert_fusion.2, pred[128,512]{0,1:T(8,128)(4,1)S(1)} %compare_and_fusion.2), kind=kLoop, calls=%fused_computation.12.clone.1 | loop fusion | flops 12058624 | bytes 5328896 | tf_op jit(solution)/shard_map/while/body/eval_jaxpr/convert_element_type | solution.py:56
  108.5 1.3 constant_dynamic-slice_fusion.3
  110.1 3.0 %fusion.93 = (f32[8,128]{1,0:T(8,128)S(1)}, f32[8,128,512]{1,2,0:T(8,128)S(1)}, f32[8,512,128]{2,1,0:T(8,128)}) fusion(f32[8,512]{1,0:T(8,128)S(1)} %dynamic-slice_convert_fusion.2, pred[128,512]{0,1:T(8,128)(4,1)S(1)} %compare_and_fusion.2, bf16[512,8,64]{0,2,1:T(8,128)(2,1)S(1)} %bitcast.116, bf16[128,8,64]{0,2,1:T(8,128)(2,1)S(1)} %get-tuple-element.292), kind=kOutput, calls=%fused_computation.39.clone.1 | convolution fusion | flops 72875008 | bytes 4935680 | tf_op jit(solution)/shard_map/while/body/eval_jaxpr/qhd,khd->hqk/dot_general | solution.py:43
  113.1 5.0 %fusion.94 = f32[8,128,4,128]{1,0,3,2:T(8,128)S(1)} fusion(f32[8,128,4,128]{1,3,2,0:T(8,128)S(1)} %bitcast.114), kind=kOutput, calls=%fused_computation.23.clone.1 | output fusion | flops 66584576 | bytes 4194304 | tf_op jit(solution)/shard_map/reduce-window.6
  118.3 1.7 copy.38
  120.0 4.8 %fusion.97 = bf16[8,128,512]{1,2,0:T(8,128)(2,1)S(1)} fusion(f32[8,128,4,128]{1,3,2,0:T(8,128)} %copy.38, f32[8,512,128]{2,1,0:T(8,128)} %get-tuple-element.259, f32[8,128]{1,0:T(8,128)S(1)} %get-tuple-element.261, f32[8,512]{1,0:T(8,128)S(1)} %dynamic-slice_convert_fusion.2, pred[128,512]{0,1:T(8,128)(4,1)S(1)} %compare_and_fusion.2), kind=kLoop, calls=%fused_computation.12.clone.1 | loop fusion | flops 12058624 | bytes 5328896 | tf_op jit(solution)/shard_map/while/body/eval_jaxpr/convert_element_type | solution.py:56
  125.2 2.9 %convolution_convert_fusion.1 = bf16[128,2048]{1,0:T(8,128)(2,1)} fusion(bf16[128,512]{0,1:T(8,128)(2,1)S(1)} %bitcast.118, bf16[512,2048]{1,0:T(8,128)(2,1)} %param.23), kind=kOutput, calls=%fused_computation.41 | convolution fusion | flops 268697600 | bytes 2752512 | tf_op jit(solution)/shard_map/dot_general | solution.py:114
  128.9 1.4 scatter_custom_fusion
  130.3 2.2 scatter_custom_fusion.1
  133.3 15.6 %reduce-scatter.3.cloned.1.call-done = bf16[128,512]{1,0:T(8,128)(2,1)} async-done(((bf16[128,2048]{1,0:T(8,128)(2,1)}), bf16[128,512]{1,0:T(8,128)(2,1)}) %reduce-scatter.3.cloned.1.call-update) | async-done | bytes 131088 | tf_op jit(solution)/shard_map/reduce_scatter | solution.py:134
  148.9 1.1 fusion.53
  150.0 5.8 %psum.7 = f32[128]{0:T(128)S(1)} all-reduce(f32[128]{0:T(128)S(1)} %get-tuple-element.193), channel_id=1, replica_groups=mesh['sp'=8,'tp'=4] {'tp'}, use_global_device_ids=true, to_apply=%region_9.10 | all-reduce | flops 128 | bytes 1024 | tf_op jit(solution)/shard_map/psum | solution.py:141
  155.9 2.0 gather_fusion
  158.0 16.3 %all_to_all.10 = bf16[8,40,512]{2,1,0:T(8,128)(2,1)} all-to-all(bf16[8,40,512]{2,1,0:T(8,128)(2,1)S(1)} %broadcast_multiply_fusion), channel_id=1, replica_groups=mesh['sp'=8,'tp'=4] {'sp'}, dimensions={0} | all-to-all | bytes 655360 | tf_op jit(solution)/shard_map/all_to_all | solution.py:148
  174.6 15.6 %all-gather.8.cloned.1.call-done = bf16[8,40,2048]{2,1,0:T(8,128)(2,1)} async-done(((bf16[8,40,512]{2,1,0:T(8,128)(2,1)}), bf16[8,40,2048]{2,1,0:T(8,128)(2,1)}) %all-gather.8.cloned.1.call-update) | async-done | bytes 1310736 | tf_op jit(solution)/shard_map/all_gather | solution.py:147
  190.1 2.8 %fusion.33 = f32[8,40,512]{2,1,0:T(8,128)S(1)} fusion(bf16[8,40,2048]{2,1,0:T(8,128)(2,1)} %all-gather.8.cloned.1.call-done, bf16[1,2048,512]{2,1,0:T(8,128)(2,1)} %param.27), kind=kOutput, calls=%fused_computation.50 | convolution fusion | flops 671252480 | bytes 4063232 | tf_op jit(solution)/shard_map/scd,df->scf/dot_general | solution.py:153
  193.0 4.8 %convolution_convert_fusion = bf16[8,40,2048]{2,1,0:T(8,128)(2,1)} fusion(bf16[1,512,2048]{2,1,0:T(8,128)(2,1)S(1)} %copy-done, bf16[8,40,2048]{2,1,0:T(8,128)(2,1)} %all-gather.8.cloned.1.call-done, bf16[1,2048,512]{2,1,0:T(8,128)(2,1)} %param.28, f32[8,40,512]{2,1,0:T(8,128)S(1)} %fusion.33), kind=kOutput, calls=%fused_computation.40 | convolution fusion | flops 1344307200 | bytes 7471104 | tf_op jit(solution)/shard_map/scf,fd->scd/dot_general | solution.py:156
  197.8 26.6 %reduce-scatter.5.cloned.1.call-done = bf16[8,40,512]{2,1,0:T(8,128)(2,1)} async-done(((bf16[8,40,2048]{2,1,0:T(8,128)(2,1)}), bf16[8,40,512]{2,1,0:T(8,128)(2,1)}) %reduce-scatter.5.cloned.1.call-update) | async-done | bytes 327696 | tf_op jit(solution)/shard_map/reduce_scatter | solution.py:157
  224.4 5.5 %all-to-all-start.1 = ((bf16[8,40,512]{2,1,0:T(8,128)(2,1)}), bf16[8,40,512]{2,1,0:T(8,128)(2,1)S(1)}, u32[]{:S(2)}, u32[]{:S(2)}) async-start(bf16[8,40,512]{2,1,0:T(8,128)(2,1)} %reduce-scatter.5.cloned.1.call-done), calls=%async_computation.3 | async-start | bytes 655360 | tf_op jit(solution)/shard_map/all_to_all | solution.py:158
  230.0 10.0 %all-to-all-done.1 = bf16[8,40,512]{2,1,0:T(8,128)(2,1)S(1)} async-done(((bf16[8,40,512]{2,1,0:T(8,128)(2,1)}), bf16[8,40,512]{2,1,0:T(8,128)(2,1)S(1)}, u32[]{:S(2)}, u32[]{:S(2)}) %all-to-all-start.1) | async-done | bytes 327712 | tf_op jit(solution)/shard_map/all_to_all | solution.py:158
  240.1 1.2 gather_fusion.1
  (74 shorter events, 9.5 us)
Async XLA Ops:
  6.5 186.5 %copy-start = (bf16[1,512,2048]{2,1,0:T(8,128)(2,1)S(1)}, bf16[1,512,2048]{2,1,0:T(8,128)(2,1)}, u32[]{:S(2)}) copy-start(bf16[1,512,2048]{2,1,0:T(8,128)(2,1)} %param.29) | copy-start | bytes 6291460
  6.5 45.1 %all-gather.6.cloned.1.call-start = ((), (), s32[]{:S(2)}) async-start(), calls=%async_computation.5 | async-start | bytes 1179648 | tf_op jit(solution)/shard_map/all_gather | solution.py:92
  9.3 82.6 %all-gather.4.cloned.1.call-start = ((), (), s32[]{:S(2)}) async-start(), calls=%async_computation.4 | async-start | bytes 1179648 | tf_op jit(solution)/shard_map/all_gather | solution.py:93
  11.1 137.9 %reduce-scatter.3.cloned.1.call-start = ((), (), s32[]{:S(2)}) async-start(), calls=%async_computation.6 | async-start | bytes 655360 | tf_op jit(solution)/shard_map/reduce_scatter | solution.py:134
  125.1 3.4 %copy-start.1 = (s32[128,2]{0,1:T(2,128)S(1)}, s32[128,2]{0,1:T(2,128)}, u32[]{:S(2)}) copy-start(s32[128,2]{0,1:T(2,128)} %param.25) | copy-start | bytes 3076
  128.1 62.1 %all-gather.8.cloned.1.call-start = ((), (), s32[]{:S(2)}) async-start(), calls=%async_computation.7 | async-start | bytes 1638400 | tf_op jit(solution)/shard_map/all_gather | solution.py:147
  174.4 50.0 %reduce-scatter.5.cloned.1.call-start = ((), (), s32[]{:S(2)}) async-start(), calls=%async_computation.8 | async-start | bytes 1638400 | tf_op jit(solution)/shard_map/reduce_scatter | solution.py:157
  193.0 36.9 %copy-start.2 = (f32[128,2]{0,1:T(2,128)S(1)}, f32[128,2]{0,1:T(2,128)}, u32[]{:S(2)}) copy-start(f32[128,2]{0,1:T(2,128)} %param.26) | copy-start | bytes 3076
  224.4 15.7 %all-to-all-start.1 = ((bf16[8,40,512]{2,1,0:T(8,128)(2,1)}), bf16[8,40,512]{2,1,0:T(8,128)(2,1)S(1)}, u32[]{:S(2)}, u32[]{:S(2)}) async-start(bf16[8,40,512]{2,1,0:T(8,128)(2,1)} %reduce-scatter.5.cloned.1.call-done), calls=%async_computation.3 | async-start | bytes 655360 | tf_op jit(solution)/shard_map/all_to_all | solution.py:158
Sparse Core Ops, SparseCore 0:
  9.4 42.1 all-gather.5
  53.6 38.1 all-gather.3
  128.2 20.6 reduce-scatter.2
  174.5 15.6 all-gather.7
  197.9 26.4 reduce-scatter.4
where the time goes:
time: 250 us; the launch traced here: 249 us
  waiting for transfers between devices  117 us (47%)
  blocking collectives  50.3 us (20%)
  other arithmetic  25.5 us (10%)
  local copies, waits for them, and re-layouts  20.1 us (8%)
  matrix products  17.2 us (7%)
  between operations  13.4 us (5%)
  starting transfers between devices  5.86 us (2%)
    all_gather x1, waiting for transfers between devices, per_device(): lax.all_gather(values, 'sp', axis=0, tiled=True)  40.3 us
    all_gather x1, blocking collectives, per_device(): lax.all_gather(stick_bias, 'sp', axis=1, tiled=True)  28.2 us
    reduce_scatter x1, waiting for transfers between devices, per_device(): lax.psum_scatter(share.astype(jnp.bfloat16), 'tp', scatter_dimension=2, t...  26.6 us
    all_to_all x1, blocking collectives, per_device(): lax.all_to_all(outgoing, 'sp', split_axis=0, concat_axis=0, tiled=True)  16.3 us
    reduce_scatter x1, waiting for transfers between devices, per_device(): lax.psum_scatter(partial_value.astype(jnp.bfloat16), 'tp', scatter_dimens...  15.6 us
    all_gather x1, waiting for transfers between devices, per_device(): lax.all_gather(lax.all_to_all(outgoing, 'sp', split_axis=0, concat_axis=0...  15.6 us
    another operation x6, other arithmetic  10.7 us
    all_to_all x1, waiting for transfers between devices, per_device(): lax.all_to_all(returned, 'sp', split_axis=0, concat_axis=0, tiled=True)  10 us
  transfers between devices with their start and end apart: 6, of which 6 were waited for; matrix products, arithmetic and copies ran while one was open for 4% of the time, Pallas kernels for 0%

commit v1 on v0

--- a/solution.py
+++ b/solution.py
@@ -1,8 +1,11 @@
+import functools
 import math
 
 import jax
 import jax.numpy as jnp
 from jax import lax
+from jax.experimental import pallas as pl
+from jax.experimental.pallas import tpu as pltpu
 from jax.sharding import PartitionSpec as P
 
 epsilon = 1e-06
@@ -163,6 +166,533 @@
     return (own_cols + routed).astype(jnp.bfloat16)
 
 
+f32 = jnp.float32
+bf16 = jnp.bfloat16
+MESH = pl.DeviceIdType.MESH
+
+
+def fused_kernel(
+    dims,
+    q_ref,
+    k_ref,
+    v_ref,
+    bias_ref,
+    qg_ref,
+    kg_ref,
+    ng_ref,
+    ids_ref,
+    rw_ref,
+    res_hbm,
+    ow_hbm,
+    gw_hbm,
+    uw_hbm,
+    dw_hbm,
+    out_ref,
+    res_v,
+    ow_v,
+    gw_v,
+    uw_v,
+    dw_v,
+    pack_s,
+    pack_r,
+    kn_v,
+    vn_v,
+    att_s,
+    att_r,
+    mix_s,
+    mix_r,
+    mix_as,
+    mix_ar,
+    disp_s,
+    x_v,
+    z_v,
+    keep_v,
+    rs_s,
+    rs_r,
+    rs_as,
+    rs_ar,
+    ret_s,
+    ret_r,
+    w_sem,
+    pack_ss,
+    pack_rs,
+    att_ss,
+    att_rs,
+    mix_ss,
+    mix_rs,
+    disp_ss,
+    x_rs,
+    fwd_ss,
+    rs_ss,
+    rs_rs,
+    ret_ss,
+    ret_rs,
+):
+    n_sp, n_tp, tok, hd, cap, own = dims
+    me = lax.axis_index("sp")
+    t = lax.axis_index("tp")
+    sib = t + 1 - 2 * (t % 2)
+    acr = (t + 2) % n_tp
+    far = (sib + 2) % n_tp
+    width = n_tp * own
+
+    def send(src, dst, ss, rs, sp_id, tp_id):
+        return pltpu.make_async_remote_copy(
+            src_ref=src,
+            dst_ref=dst,
+            send_sem=ss,
+            recv_sem=rs,
+            device_id=(sp_id, tp_id),
+            device_id_type=MESH,
+        )
+
+    def cols(index):
+        return pl.ds(pl.multiple_of(index * own, own), own)
+
+    loads = [
+        pltpu.make_async_copy(ow_hbm, ow_v, w_sem.at[0]),
+        pltpu.make_async_copy(res_hbm.at[:, cols(t)], res_v, w_sem.at[1]),
+        pltpu.make_async_copy(gw_hbm.at[0], gw_v, w_sem.at[2]),
+        pltpu.make_async_copy(uw_hbm.at[0], uw_v, w_sem.at[3]),
+        pltpu.make_async_copy(dw_hbm.at[0], dw_v, w_sem.at[4]),
+    ]
+    for load in loads:
+        load.start()
+
+    barrier = pltpu.get_barrier_semaphore()
+    for d in range(1, n_sp):
+        pl.semaphore_signal(
+            barrier, inc=1, device_id=((me + d) % n_sp, t), device_id_type=MESH
+        )
+    for peer in (sib, acr):
+        pl.semaphore_signal(barrier, inc=1, device_id=(me, peer), device_id_type=MESH)
+
+    half = tok // 2
+    for h in range(n_sp):
+        lanes = slice(h * hd, (h + 1) * hd)
+        q_h = q_ref[:, lanes].astype(f32)
+        k_h = k_ref[:, lanes].astype(f32)
+        v_h = v_ref[:, lanes].astype(f32)
+        pack_s[h, 0:tok, :] = jnp.concatenate([q_h, k_h], axis=1).astype(bf16)
+        pack_s[h, tok : tok + half, :] = jnp.concatenate([v_h[:half], v_h[half:]], axis=1).astype(
+            bf16
+        )
+        pack_s[h, tok + half : tok + half + 16, :] = jnp.broadcast_to(
+            bias_ref[h : h + 1, :].astype(f32), (16, tok)
+        ).astype(bf16)
+    pl.semaphore_wait(barrier, n_sp + 1)
+
+    def pack_copy(block, peer, slot):
+        return send(
+            pack_s.at[block], pack_r.at[slot], pack_ss.at[block], pack_rs.at[slot], peer, t
+        )
+
+    for d in range(1, n_sp):
+        peer = (me + d) % n_sp
+        pack_copy(peer, peer, me).start()
+    pack_r[me] = pack_s[me]
+
+    ids0 = ids_ref[:, 0:1]
+    ids1 = ids_ref[:, 1:2]
+    lane = lax.broadcasted_iota(jnp.int32, (tok, 128), 1)
+    row = lax.broadcasted_iota(jnp.int32, (tok, tok), 0)
+    col = lax.broadcasted_iota(jnp.int32, (tok, tok), 1)
+    named0 = (lane == ids0).astype(f32)
+    named1 = (lane == ids1).astype(f32)
+    earlier = (col < row).astype(f32).astype(bf16)
+    count = jnp.dot(earlier, (named0 + named1).astype(bf16), preferred_element_type=f32)
+    slot0 = jnp.sum(named0 * count, axis=1, keepdims=True) + (ids0 * cap).astype(f32)
+    slot1 = jnp.sum(named1 * count, axis=1, keepdims=True) + (ids1 * cap).astype(f32)
+    slots = lax.broadcasted_iota(jnp.int32, (tok, n_sp * cap), 1).astype(f32)
+    pick0 = (slots == slot0).astype(f32)
+    pick1 = (slots == slot1).astype(f32)
+
+    qb = 2 * tok
+    row = lax.broadcasted_iota(jnp.int32, (qb, qb), 0)
+    col = lax.broadcasted_iota(jnp.int32, (qb, qb), 1)
+    causal = col < row
+    tri = (row >= col).astype(f32).astype(bf16)
+    bias_rows = []
+    for i in range(n_sp // 2):
+        blocks = []
+        v_blocks = []
+        bias_i = []
+        for b in (2 * i, 2 * i + 1):
+
+            @pl.when(b != me)
+            def _():
+                pack_copy(b, b, b).wait_recv()
+
+            blocks.append(pack_r[b, 0:tok, :].astype(f32))
+            vp = pack_r[b, tok : tok + half, :].astype(f32)
+            v_blocks += [vp[:, :hd], vp[:, hd:]]
+            bias_i.append(pack_r[b, tok + half : tok + half + 16, :].astype(f32)[0:1])
+        both = jnp.concatenate(blocks, axis=0)
+        q_i = both[:, :hd]
+        k_i = both[:, hd:]
+        q_i = q_i * lax.rsqrt(jnp.mean(q_i * q_i, axis=1, keepdims=True) + epsilon) * qg_ref[...]
+        k_i = k_i * lax.rsqrt(jnp.mean(k_i * k_i, axis=1, keepdims=True) + epsilon) * kg_ref[...]
+        q_n = (q_i.astype(bf16).astype(f32) * hd**-0.5).astype(bf16)
+        kn_v[i] = k_i.astype(bf16)
+        vn_v[i] = jnp.concatenate(v_blocks, axis=0).astype(bf16)
+        bias_rows.append(jnp.concatenate(bias_i, axis=1))
+        summed = jnp.zeros((qb, hd), f32)
+        carry = jnp.zeros((qb, 1), f32)
+        for j in range(i, -1, -1):
+            s = lax.dot_general(
+                q_n, kn_v[j], (((1,), (1,)), ((), ())), preferred_element_type=f32
+            )
+            s = s - bias_rows[j]
+            leave = jnp.maximum(s, 0.0) + jnp.log(1.0 + jnp.exp(-jnp.abs(s)))
+            if j == i:
+                leave = jnp.where(causal, leave, 0.0)
+            top = leave.astype(bf16)
+            low = (leave - top.astype(f32)).astype(bf16)
+            total = jnp.dot(top, tri, preferred_element_type=f32) + jnp.dot(
+                low, tri, preferred_element_type=f32
+            )
+            weight = jnp.exp(s - total - carry)
+            if j == i:
+                weight = jnp.where(causal, weight, 0.0)
+            carry = carry + total[:, 0:1]
+            summed = summed + jnp.dot(weight.astype(bf16), vn_v[j], preferred_element_type=f32)
+        for b in (2 * i, 2 * i + 1):
+            part = summed[(b - 2 * i) * tok : (b - 2 * i + 1) * tok]
+            packed = jnp.concatenate([part[:half], part[half:]], axis=1).astype(bf16)
+            att_s[b] = packed
+
+            @pl.when(b != me)
+            def _():
+                send(att_s.at[b], att_r.at[me], att_ss.at[b], att_rs.at[me], b, t).start()
+
+            @pl.when(b == me)
+            def _():
+                att_r[b] = packed
+
+    for h in range(n_sp):
+
+        @pl.when(h != me)
+        def _():
+            send(att_s.at[h], att_r.at[h], att_ss.at[h], att_rs.at[h], h, t).wait_recv()
+
+    heads = []
+    for h in range(n_sp):
+        p = att_r[h].astype(f32)
+        heads.append(jnp.concatenate([p[:, :hd], p[:, hd:]], axis=0))
+    attended = jnp.concatenate(heads, axis=1).astype(bf16)
+
+    loads[0].wait()
+
+    def project(index):
+        return jnp.dot(attended, ow_v[:, cols(index)], preferred_element_type=f32)
+
+    def mix_copy(slot):
+        return send(mix_s.at[slot], mix_r.at[slot], mix_ss.at[slot], mix_rs.at[slot], me, sib)
+
+    mix_s[1] = project(far).astype(bf16)
+    mix_copy(1).start()
+    mix_s[0] = project(sib).astype(bf16)
+    mix_copy(0).start()
+    across = project(acr)
+    mix_copy(1).wait_recv()
+    mix_as[...] = (across + mix_r[1].astype(f32)).astype(bf16)
+    mix_over = send(mix_as, mix_ar, mix_ss.at[2], mix_rs.at[2], me, acr)
+    mix_over.start()
+    mixed = project(t)
+    loads[1].wait()
+    mix_copy(0).wait_recv()
+    mixed = mixed + mix_r[0].astype(f32) + res_v[...].astype(f32)
+    mix_over.wait_recv()
+    own_b = (mixed + mix_ar[...].astype(f32)).astype(bf16)
+
+    spread = lax.dot_general(
+        (pick0 + pick1).astype(bf16), own_b, (((0,), (0,)), ((), ())), preferred_element_type=f32
+    )
+    for e in range(n_sp):
+        disp_s[e] = spread[e * cap : (e + 1) * cap].astype(bf16)
+
+    quad = n_sp // 2
+    base_near = (me // quad) * quad
+    base_away = (base_near + quad) % n_sp
+
+    def disp_copy(block, peer, slot):
+        return send(
+            disp_s.at[block], x_v.at[t, slot], disp_ss.at[block], x_rs.at[t, slot], peer, t
+        )
+
+    away = [base_away + (me + g) % quad for g in range(quad)]
+    near = [base_near + (me + g) % quad for g in range(quad)]
+    order = []
+    for g in range(1, quad):
+        order += [near[g], away[g]]
+    for peer in order + [away[0]]:
+        disp_copy(peer, peer, me).start()
+    x_v[t, me] = disp_s[me]
+
+    def pass_sib(column, src, sem):
+        return send(
+            x_v.at[column, src],
+            x_v.at[column, src],
+            fwd_ss.at[sem, src],
+            x_rs.at[column, src],
+            me,
+            sib,
+        )
+
+    def pass_acr(src):
+        return send(x_v.at[t, src], x_v.at[t, src], fwd_ss.at[1, src], x_rs.at[t, src], me, acr)
+
+    def came(column, src):
+        send(
+            x_v.at[column, src], x_v.at[column, src], fwd_ss.at[0, src], x_rs.at[column, src], me, sib
+        ).wait_recv()
+
+    def first_pass(srcs, skip_first):
+        for g, src in enumerate(srcs):
+            if not (skip_first and g == 0):
+                came(t, src)
+            pass_acr(src).start()
+            pass_sib(t, src, 0).start()
+
+    def second_pass(srcs):
+        for src in srcs:
+            came(acr, src)
+            pass_sib(acr, src, 2).start()
+
+    def expert_share(group, srcs):
+        for src in srcs:
+            came(sib, src)
+            came(far, src)
+        base = base_near if group == 0 else base_away
+        pieces = []
+        for g in range(quad):
+            pieces.append(
+                jnp.concatenate([x_v[c, base + g].astype(f32) for c in range(n_tp)], axis=1)
+            )
+        rows = jnp.concatenate(pieces, axis=0)
+        scale = lax.rsqrt(jnp.mean(rows * rows, axis=1, keepdims=True) + epsilon)
+        z_v[...] = (rows * scale * ng_ref[...]).astype(bf16)
+        if group == 0:
+            loads[2].wait()
+            loads[3].wait()
+        gate_pre = jnp.dot(z_v[...], gw_v[...], preferred_element_type=f32)
+        up_pre = jnp.dot(z_v[...], uw_v[...], preferred_element_type=f32)
+        hidden = activate(gate_pre, up_pre).astype(bf16)
+        if group == 0:
+            loads[4].wait()
+
+        def down(index):
+            return jnp.dot(hidden, dw_v[:, cols(index)], preferred_element_type=f32)
+
+        rs_s[group, 1] = down(far).astype(bf16)
+        rs_copy(group, 1).start()
+        rs_s[group, 0] = down(sib).astype(bf16)
+        rs_copy(group, 0).start()
+        keep_v[group, 1] = down(acr)
+        keep_v[group, 0] = down(t)
+
+    def rs_copy(group, slot):
+        return send(
+            rs_s.at[group, slot],
+            rs_r.at[group, slot],
+            rs_ss.at[group, slot],
+            rs_rs.at[group, slot],
+            me,
+            sib,
+        )
+
+    def rs_over(group):
+        return send(
+            rs_as.at[group], rs_ar.at[group], rs_ss.at[group, 2], rs_rs.at[group, 2], me, acr
+        )
+
+    def step_over(group):
+        rs_copy(group, 1).wait_recv()
+        rs_as[group] = (keep_v[group, 1] + rs_r[group, 1].astype(f32)).astype(bf16)
+        rs_over(group).start()
+
+    def ret_copy(block, peer, slot):
+        return send(ret_s.at[block], ret_r.at[slot], ret_ss.at[block], ret_rs.at[slot], peer, t)
+
+    def step_back(group):
+        rs_copy(group, 0).wait_recv()
+        part = keep_v[group, 0] + rs_r[group, 0].astype(f32)
+        rs_over(group).wait_recv()
+        part = part + rs_ar[group].astype(f32)
+        base = base_near if group == 0 else base_away
+        for g in range(quad):
+            src = base + g
+            rows = part[g * cap : (g + 1) * cap].astype(bf16)
+            ret_s[src] = rows
+            if group == 0:
+
+                @pl.when(src != me)
+                def _():
+                    ret_copy(src, src, me).start()
+
+                @pl.when(src == me)
+                def _():
+                    ret_r[src] = rows
+
+            else:
+                ret_copy(src, src, me).start()
+
+    first_pass(near, True)
+    second_pass(near)
+    first_pass(away, False)
+    expert_share(0, near)
+    second_pass(away)
+    step_over(0)
+    expert_share(1, away)
+    step_back(0)
+    step_over(1)
+    step_back(1)
+
+    for d in range(1, n_sp):
+        src = (me + d) % n_sp
+        ret_copy(src, src, src).wait_recv()
+    back = jnp.concatenate([ret_r[e].astype(f32) for e in range(n_sp)], axis=0).astype(bf16)
+    taken0 = jnp.dot(pick0.astype(bf16), back, preferred_element_type=f32)
+    taken1 = jnp.dot(pick1.astype(bf16), back, preferred_element_type=f32)
+    routed = taken0 * rw_ref[:, 0:1] + taken1 * rw_ref[:, 1:2]
+    out_ref[...] = (own_b.astype(f32) + routed).astype(bf16)
+
+    for d in range(1, n_sp):
+        peer = (me + d) % n_sp
+        pack_copy(peer, peer, me).wait_send()
+        send(att_s.at[peer], att_r.at[me], att_ss.at[peer], att_rs.at[me], peer, t).wait_send()
+        disp_copy(peer, peer, me).wait_send()
+        ret_copy(peer, peer, me).wait_send()
+    mix_copy(0).wait_send()
+    mix_copy(1).wait_send()
+    mix_over.wait_send()
+    for src in range(n_sp):
+        pass_acr(src).wait_send()
+        pass_sib(t, src, 0).wait_send()
+        pass_sib(acr, src, 2).wait_send()
+    for group in range(2):
+        rs_copy(group, 0).wait_send()
+        rs_copy(group, 1).wait_send()
+        rs_over(group).wait_send()
+
+
+def fused_device(n_sp, n_tp, *args):
+    (
+        residual,
+        queries,
+        keys,
+        values,
+        stick_bias,
+        query_gain,
+        key_gain,
+        out_weight,
+        norm_gain,
+        route_ids,
+        route_weights,
+        gate_weight,
+        up_weight,
+        down_weight,
+    ) = args
+    tok, packed = queries.shape
+    hd = query_gain.shape[0]
+    model = residual.shape[1]
+    own = model // n_tp
+    hidden = gate_weight.shape[2]
+    picks = route_ids.shape[1]
+    cap = (5 * tok * picks + 4 * n_sp - 1) // (4 * n_sp)
+    quad = n_sp // 2
+    pairs = n_sp // 2
+    half = tok // 2
+    vmem = pl.BlockSpec(memory_space=pltpu.VMEM)
+    anywhere = pl.BlockSpec(memory_space=pl.ANY)
+    dma = pltpu.SemaphoreType.DMA
+    scratch = [
+        pltpu.VMEM((tok, own), bf16),
+        pltpu.VMEM((packed, model), bf16),
+        pltpu.VMEM((model, hidden), bf16),
+        pltpu.VMEM((model, hidden), bf16),
+        pltpu.VMEM((hidden, model), bf16),
+        pltpu.VMEM((n_sp, tok + half + 16, 2 * hd), bf16),
+        pltpu.VMEM((n_sp, tok + half + 16, 2 * hd), bf16),
+        pltpu.VMEM((pairs, 2 * tok, hd), bf16),
+        pltpu.VMEM((pairs, 2 * tok, hd), bf16),
+        pltpu.VMEM((n_sp, half, 2 * hd), bf16),
+        pltpu.VMEM((n_sp, half, 2 * hd), bf16),
+        pltpu.VMEM((2, tok, own), bf16),
+        pltpu.VMEM((2, tok, own), bf16),
+        pltpu.VMEM((tok, own), bf16),
+        pltpu.VMEM((tok, own), bf16),
+        pltpu.VMEM((n_sp, cap, own), bf16),
+        pltpu.VMEM((n_tp, n_sp, cap, own), bf16),
+        pltpu.VMEM((quad * cap, model), bf16),
+        pltpu.VMEM((2, 2, quad * cap, own), f32),
+        pltpu.VMEM((2, 2, quad * cap, own), bf16),
+        pltpu.VMEM((2, 2, quad * cap, own), bf16),
+        pltpu.VMEM((2, quad * cap, own), bf16),
+        pltpu.VMEM((2, quad * cap, own), bf16),
+        pltpu.VMEM((n_sp, cap, own), bf16),
+        pltpu.VMEM((n_sp, cap, own), bf16),
+        dma((5,)),
+        dma((n_sp,)),
+        dma((n_sp,)),
+        dma((n_sp,)),
+        dma((n_sp,)),
+        dma((3,)),
+        dma((3,)),
+        dma((n_sp,)),
+        dma((n_tp, n_sp)),
+        dma((3, n_sp)),
+        dma((2, 3)),
+        dma((2, 3)),
+        dma((n_sp,)),
+        dma((n_sp,)),
+    ]
+    return pl.pallas_call(
+        functools.partial(fused_kernel, (n_sp, n_tp, tok, hd, cap, own)),
+        out_shape=jax.ShapeDtypeStruct((tok, own), bf16),
+        in_specs=[vmem] * 9 + [anywhere] * 5,
+        out_specs=vmem,
+        scratch_shapes=scratch,
+        compiler_params=pltpu.CompilerParams(
+            collective_id=0, has_side_effects=True, vmem_limit_bytes=56 * 1024 * 1024
+        ),
+    )(
+        queries,
+        keys,
+        values,
+        stick_bias,
+        query_gain.reshape(1, -1),
+        key_gain.reshape(1, -1),
+        norm_gain.reshape(1, -1),
+        route_ids,
+        route_weights,
+        residual,
+        out_weight,
+        gate_weight,
+        up_weight,
+        down_weight,
+    )
+
+
+def device_program(n_sp, n_tp, *args):
+    tok, packed = args[1].shape
+    hd = args[5].shape[0]
+    picks = args[9].shape[1]
+    cap = (5 * tok * picks + 4 * n_sp - 1) // (4 * n_sp)
+    fits = (
+        packed == n_sp * hd
+        and tok == 2 * hd == 128
+        and cap % 8 == 0
+        and n_tp == 4
+        and n_sp % 4 == 0
+        and picks == 2
+        and args[11].shape[0] == 1
+    )
+    if fits:
+        return fused_device(n_sp, n_tp, *args)
+    return per_device(*args)
+
+
 def solution(mesh):
     placed = (
         P("sp", None),
@@ -181,5 +711,6 @@
         P("sp", "tp", None),
     )
     return jax.shard_map(
-        per_device, mesh=mesh, in_specs=placed, out_specs=P("sp", "tp"), check_vma=False
-    )
+        functools.partial(device_program, mesh.shape["sp"], mesh.shape["tp"]),
+        mesh=mesh, in_specs=placed, out_specs=P("sp", "tp"), check_vma=False
+    )

time: 250 us -> 68.3 us (0.27)
  waiting for transfers between devices: 117 us -> 0 us
  Pallas kernels: 0 us -> 63.7 us
  blocking collectives: 50.3 us -> 0 us
  other arithmetic: 25.5 us -> 0 us
  matrix products: 17.2 us -> 0 us
  local copies, waits for them, and re-layouts: 20.1 us -> 4.38 us
  between operations: 13.4 us -> 0.01 us
  starting transfers between devices: 5.86 us -> 0 us
    all_gather x3 -> x0, waiting for transfers between devices: 64.7 us -> none  [the longest x1 40.3 us: per_device(): lax.all_gather(values, 'sp', axis=0, tiled=True)]
    pallas_call x0 -> x1, Pallas kernels: none -> 63.7 us  [fused_device(): pl.pallas_call(functools.partial(fused_kernel, (n_sp, n_tp, tok, hd, cap,...]
    reduce_scatter x2 -> x0, waiting for transfers between devices: 42.2 us -> none  [the longest x1 26.6 us: per_device(): lax.psum_scatter(share.astype(jnp.bfloat16), 'tp', scatter_dimension=2, t...]
    all_gather x1 -> x0, blocking collectives: 28.2 us -> none  [per_device(): lax.all_gather(stick_bias, 'sp', axis=1, tiled=True)]
    dot_general x7 -> x0, matrix products: 17.2 us -> none  [the longest x2 6.02 us: key_block(): jnp.einsum('qhd,khd->hqk', queries_n, keys_heads, preferred_element_type=...]
    all_to_all x1 -> x0, blocking collectives: 16.3 us -> none  [per_device(): lax.all_to_all(outgoing, 'sp', split_axis=0, concat_axis=0, tiled=True)]
    convert_element_type x10 -> x0, other arithmetic: 12 us -> none  [the longest x2 9.63 us: key_block(): weight.astype(jnp.bfloat16)]
    another operation x8 -> x0, other arithmetic: 11 us -> none
  transfers between devices with their start and end apart: 6 -> 0, of which waited for: 6 -> 0; matrix products, arithmetic and copies ran while one was open for 4% -> 0% of each run, Pallas kernels for 0% -> 0%
where the time goes in v1:
time: 68.3 us; the launch traced here: 68.1 us
  Pallas kernels  63.7 us (93%)
  local copies, waits for them, and re-layouts  4.38 us (6%)
    pallas_call x1, Pallas kernels, fused_device(): pl.pallas_call(functools.partial(fused_kernel, (n_sp, n_tp, tok, hd, cap,...  63.7 us
    unnamed x3, local copies, waits for them, and re-layouts  4.38 us

profile of v1, /device:TPU:0, one launch (start us, length us, event | category | flops | bytes accessed | tf_op | source)
XLA Modules:
  0.0 68.1 jit_solution(14806061647938333099)
XLA Ops:
  0.0 1.4 %copy.15.ids_ref = s32[128,2]{1,0:T(8,128)} copy(s32[128,2]{0,1:T(2,128)} %param.23) | data formatting | bytes 2048 | tf_op args[9]
  1.4 1.4 %copy.16.rw_ref = f32[128,2]{1,0:T(8,128)} copy(f32[128,2]{0,1:T(2,128)} %param.24) | data formatting | bytes 2048 | tf_op args[10]
  2.8 63.7 %shard_map.136 = bf16[128,512]{1,0:T(8,128)(2,1)} custom-call(bf16[128,512]{1,0:T(8,128)(2,1)} %q_ref.1, bf16[128,512]{1,0:T(8,128)(2,1)} %k_ref.1, bf16[128,512]{1,0:T(8,128)(2,1)} %v_ref.1, bf16[8,128]{1,0:T(8,128)(2,1)} %bias_ref.1, f32[1,64]{1,0:T(1,128)} %bitcast.4, f32[1,64]{1,0:T(1,128)} %bitcast.5, f32[1,2048]{1,0:T(1,128)} %bitcast.3, ...), custom_call_target="tpu_custom_call" | custom-call | tf_op jit(solution)/shard_map/pallas_call | solution.py:650
  66.6 1.6 %copy.18 = bf16[128,512]{1,0:T(8,128)(2,1)} copy(bf16[128,512]{1,0:T(8,128)(2,1)} %shard_map.136) | data formatting | bytes 262144

commit v2 on v1

--- a/solution.py
+++ b/solution.py
@@ -225,6 +225,8 @@
     fwd_ss,
     rs_ss,
     rs_rs,
+    over_ss,
+    over_rs,
     ret_ss,
     ret_rs,
 ):
@@ -292,17 +294,22 @@
         pack_copy(peer, peer, me).start()
     pack_r[me] = pack_s[me]
 
-    ids0 = ids_ref[:, 0:1]
-    ids1 = ids_ref[:, 1:2]
-    lane = lax.broadcasted_iota(jnp.int32, (tok, 128), 1)
+    by_token = jnp.transpose(
+        jnp.concatenate(
+            [ids_ref[...].astype(f32), rw_ref[...], jnp.zeros((4, tok), f32)], axis=0
+        )
+    )
+    ids0 = by_token[:, 0:1]
+    ids1 = by_token[:, 1:2]
+    lane = lax.broadcasted_iota(jnp.int32, (tok, 128), 1).astype(f32)
     row = lax.broadcasted_iota(jnp.int32, (tok, tok), 0)
     col = lax.broadcasted_iota(jnp.int32, (tok, tok), 1)
     named0 = (lane == ids0).astype(f32)
     named1 = (lane == ids1).astype(f32)
     earlier = (col < row).astype(f32).astype(bf16)
     count = jnp.dot(earlier, (named0 + named1).astype(bf16), preferred_element_type=f32)
-    slot0 = jnp.sum(named0 * count, axis=1, keepdims=True) + (ids0 * cap).astype(f32)
-    slot1 = jnp.sum(named1 * count, axis=1, keepdims=True) + (ids1 * cap).astype(f32)
+    slot0 = jnp.sum(named0 * count, axis=1, keepdims=True) + ids0 * cap
+    slot1 = jnp.sum(named1 * count, axis=1, keepdims=True) + ids1 * cap
     slots = lax.broadcasted_iota(jnp.int32, (tok, n_sp * cap), 1).astype(f32)
     pick0 = (slots == slot0).astype(f32)
     pick1 = (slots == slot1).astype(f32)
@@ -412,20 +419,17 @@
         disp_s[e] = spread[e * cap : (e + 1) * cap].astype(bf16)
 
     quad = n_sp // 2
-    base_near = (me // quad) * quad
-    base_away = (base_near + quad) % n_sp
+    line = me // 2
+    side = me % 2
+    lines = [line, line + 1 - 2 * (line % 2), (line + 2) % quad, quad - 1 - line]
+    groups = [[2 * at + side for at in lines], [2 * at + 1 - side for at in lines]]
 
     def disp_copy(block, peer, slot):
         return send(
             disp_s.at[block], x_v.at[t, slot], disp_ss.at[block], x_rs.at[t, slot], peer, t
         )
 
-    away = [base_away + (me + g) % quad for g in range(quad)]
-    near = [base_near + (me + g) % quad for g in range(quad)]
-    order = []
-    for g in range(1, quad):
-        order += [near[g], away[g]]
-    for peer in order + [away[0]]:
+    for peer in groups[0][1:] + groups[1]:
         disp_copy(peer, peer, me).start()
     x_v[t, me] = disp_s[me]
 
@@ -463,12 +467,9 @@
         for src in srcs:
             came(sib, src)
             came(far, src)
-        base = base_near if group == 0 else base_away
         pieces = []
-        for g in range(quad):
-            pieces.append(
-                jnp.concatenate([x_v[c, base + g].astype(f32) for c in range(n_tp)], axis=1)
-            )
+        for src in srcs:
+            pieces.append(jnp.concatenate([x_v[c, src].astype(f32) for c in range(n_tp)], axis=1))
         rows = jnp.concatenate(pieces, axis=0)
         scale = lax.rsqrt(jnp.mean(rows * rows, axis=1, keepdims=True) + epsilon)
         z_v[...] = (rows * scale * ng_ref[...]).astype(bf16)
@@ -501,49 +502,46 @@
             sib,
         )
 
-    def rs_over(group):
+    def rs_over(group, g):
         return send(
-            rs_as.at[group], rs_ar.at[group], rs_ss.at[group, 2], rs_rs.at[group, 2], me, acr
-        )
+            rs_as.at[group, g], rs_ar.at[group, g], over_ss.at[group, g], over_rs.at[group, g], me, acr
+        )
+
+    turns = (2, 3, 1, 0)
 
     def step_over(group):
         rs_copy(group, 1).wait_recv()
-        rs_as[group] = (keep_v[group, 1] + rs_r[group, 1].astype(f32)).astype(bf16)
-        rs_over(group).start()
+        for g in turns:
+            rows = slice(g * cap, (g + 1) * cap)
+            rs_as[group, g] = (keep_v[group, 1, rows] + rs_r[group, 1, rows].astype(f32)).astype(
+                bf16
+            )
+            rs_over(group, g).start()
 
     def ret_copy(block, peer, slot):
         return send(ret_s.at[block], ret_r.at[slot], ret_ss.at[block], ret_rs.at[slot], peer, t)
 
     def step_back(group):
         rs_copy(group, 0).wait_recv()
-        part = keep_v[group, 0] + rs_r[group, 0].astype(f32)
-        rs_over(group).wait_recv()
-        part = part + rs_ar[group].astype(f32)
-        base = base_near if group == 0 else base_away
-        for g in range(quad):
-            src = base + g
-            rows = part[g * cap : (g + 1) * cap].astype(bf16)
-            ret_s[src] = rows
-            if group == 0:
-
-                @pl.when(src != me)
-                def _():
-                    ret_copy(src, src, me).start()
-
-                @pl.when(src == me)
-                def _():
-                    ret_r[src] = rows
-
+        for g in turns:
+            span = slice(g * cap, (g + 1) * cap)
+            part = keep_v[group, 0, span] + rs_r[group, 0, span].astype(f32)
+            rs_over(group, g).wait_recv()
+            rows = (part + rs_ar[group, g].astype(f32)).astype(bf16)
+            src = groups[group][g]
+            if group == 0 and g == 0:
+                ret_r[src] = rows
             else:
+                ret_s[src] = rows
                 ret_copy(src, src, me).start()
 
-    first_pass(near, True)
-    second_pass(near)
-    first_pass(away, False)
-    expert_share(0, near)
-    second_pass(away)
+    first_pass(groups[0], True)
+    second_pass(groups[0])
+    first_pass(groups[1], False)
+    expert_share(0, groups[0])
+    second_pass(groups[1])
     step_over(0)
-    expert_share(1, away)
+    expert_share(1, groups[1])
     step_back(0)
     step_over(1)
     step_back(1)
@@ -554,7 +552,7 @@
     back = jnp.concatenate([ret_r[e].astype(f32) for e in range(n_sp)], axis=0).astype(bf16)
     taken0 = jnp.dot(pick0.astype(bf16), back, preferred_element_type=f32)
     taken1 = jnp.dot(pick1.astype(bf16), back, preferred_element_type=f32)
-    routed = taken0 * rw_ref[:, 0:1] + taken1 * rw_ref[:, 1:2]
+    routed = taken0 * by_token[:, 2:3] + taken1 * by_token[:, 3:4]
     out_ref[...] = (own_b.astype(f32) + routed).astype(bf16)
 
     for d in range(1, n_sp):
@@ -573,7 +571,8 @@
     for group in range(2):
         rs_copy(group, 0).wait_send()
         rs_copy(group, 1).wait_send()
-        rs_over(group).wait_send()
+        for g in range(quad):
+            rs_over(group, g).wait_send()
 
 
 def fused_device(n_sp, n_tp, *args):
@@ -628,8 +627,8 @@
         pltpu.VMEM((2, 2, quad * cap, own), f32),
         pltpu.VMEM((2, 2, quad * cap, own), bf16),
         pltpu.VMEM((2, 2, quad * cap, own), bf16),
-        pltpu.VMEM((2, quad * cap, own), bf16),
-        pltpu.VMEM((2, quad * cap, own), bf16),
+        pltpu.VMEM((2, quad, cap, own), bf16),
+        pltpu.VMEM((2, quad, cap, own), bf16),
         pltpu.VMEM((n_sp, cap, own), bf16),
         pltpu.VMEM((n_sp, cap, own), bf16),
         dma((5,)),
@@ -642,8 +641,10 @@
         dma((n_sp,)),
         dma((n_tp, n_sp)),
         dma((3, n_sp)),
-        dma((2, 3)),
-        dma((2, 3)),
+        dma((2, 2)),
+        dma((2, 2)),
+        dma((2, quad)),
+        dma((2, quad)),
         dma((n_sp,)),
         dma((n_sp,)),
     ]
@@ -664,8 +665,8 @@
         query_gain.reshape(1, -1),
         key_gain.reshape(1, -1),
         norm_gain.reshape(1, -1),
-        route_ids,
-        route_weights,
+        route_ids.T,
+        route_weights.T,
         residual,
         out_weight,
         gate_weight,
@@ -684,7 +685,7 @@
         and tok == 2 * hd == 128
         and cap % 8 == 0
         and n_tp == 4
-        and n_sp % 4 == 0
+        and n_sp == 8
         and picks == 2
         and args[11].shape[0] == 1
     )

time: 68.3 us -> 61.2 us (0.90)
  Pallas kernels: 63.7 us -> 59.4 us
  local copies, waits for them, and re-layouts: 4.38 us -> 1.57 us
    pallas_call x1, Pallas kernels: 63.7 us -> 59.4 us  [fused_device(): pl.pallas_call(functools.partial(fused_kernel, (n_sp, n_tp, tok, hd, cap,...]
    unnamed x3 -> x1, local copies, waits for them, and re-layouts: 4.38 us -> 1.57 us
where the time goes in v2:
time: 61.2 us; the launch traced here: 61 us
  Pallas kernels  59.4 us (97%)
  local copies, waits for them, and re-layouts  1.57 us (3%)
    pallas_call x1, Pallas kernels, fused_device(): pl.pallas_call(functools.partial(fused_kernel, (n_sp, n_tp, tok, hd, cap,...  59.4 us
    unnamed x1, local copies, waits for them, and re-layouts  1.57 us

profile of v2, /device:TPU:0, one launch (start us, length us, event | category | flops | bytes accessed | tf_op | source)
XLA Modules:
  0.0 61.0 jit_solution(4090252084466393747)
XLA Ops:
  0.0 59.4 %shard_map.136 = bf16[128,512]{1,0:T(8,128)(2,1)} custom-call(bf16[128,512]{1,0:T(8,128)(2,1)} %q_ref.1, bf16[128,512]{1,0:T(8,128)(2,1)} %k_ref.1, bf16[128,512]{1,0:T(8,128)(2,1)} %v_ref.1, bf16[8,128]{1,0:T(8,128)(2,1)} %bias_ref.1, f32[1,64]{1,0:T(1,128)} %bitcast.8, f32[1,64]{1,0:T(1,128)} %bitcast.9, f32[1,2048]{1,0:T(1,128)} %bitcast.5, ...), custom_call_target="tpu_custom_call" | custom-call | tf_op jit(solution)/shard_map/pallas_call | solution.py:651
  59.5 1.6 %copy.16 = bf16[128,512]{1,0:T(8,128)(2,1)} copy(bf16[128,512]{1,0:T(8,128)(2,1)} %shard_map.136) | data formatting | bytes 262144

commit v3 on v2

--- a/solution.py
+++ b/solution.py
@@ -173,10 +173,10 @@
 
 def fused_kernel(
     dims,
-    q_ref,
-    k_ref,
-    v_ref,
-    bias_ref,
+    q_hbm,
+    k_hbm,
+    v_hbm,
+    bias_hbm,
     qg_ref,
     kg_ref,
     ng_ref,
@@ -188,6 +188,14 @@
     uw_hbm,
     dw_hbm,
     out_ref,
+    q_ref,
+    k_ref,
+    v_ref,
+    bias_ref,
+    qn_v,
+    bias_v,
+    sum_v,
+    carry_v,
     res_v,
     ow_v,
     gw_v,
@@ -238,6 +246,12 @@
     far = (sib + 2) % n_tp
     width = n_tp * own
 
+    quad = n_sp // 2
+    line = me // 2
+    side = me % 2
+    lines = [line, line + 1 - 2 * (line % 2), (line + 2) % quad, quad - 1 - line]
+    groups = [[2 * at + side for at in lines], [2 * at + 1 - side for at in lines]]
+
     def send(src, dst, ss, rs, sp_id, tp_id):
         return pltpu.make_async_remote_copy(
             src_ref=src,
@@ -257,10 +271,11 @@
         pltpu.make_async_copy(gw_hbm.at[0], gw_v, w_sem.at[2]),
         pltpu.make_async_copy(uw_hbm.at[0], uw_v, w_sem.at[3]),
         pltpu.make_async_copy(dw_hbm.at[0], dw_v, w_sem.at[4]),
+        pltpu.make_async_copy(q_hbm, q_ref, w_sem.at[5]),
+        pltpu.make_async_copy(k_hbm, k_ref, w_sem.at[6]),
+        pltpu.make_async_copy(v_hbm, v_ref, w_sem.at[7]),
+        pltpu.make_async_copy(bias_hbm, bias_ref, w_sem.at[8]),
     ]
-    for load in loads:
-        load.start()
-
     barrier = pltpu.get_barrier_semaphore()
     for d in range(1, n_sp):
         pl.semaphore_signal(
@@ -268,6 +283,11 @@
         )
     for peer in (sib, acr):
         pl.semaphore_signal(barrier, inc=1, device_id=(me, peer), device_id_type=MESH)
+
+    for load in loads[5:] + loads[:5]:
+        load.start()
+    for load in loads[5:]:
+        load.wait()
 
     half = tok // 2
     for h in range(n_sp):
@@ -289,8 +309,9 @@
             pack_s.at[block], pack_r.at[slot], pack_ss.at[block], pack_rs.at[slot], peer, t
         )
 
-    for d in range(1, n_sp):
-        peer = (me + d) % n_sp
+    for peer in (
+        [groups[0][1], groups[1][1], groups[1][0]] + groups[0][2:] + groups[1][2:]
+    ):
         pack_copy(peer, peer, me).start()
     pack_r[me] = pack_s[me]
 
@@ -319,8 +340,8 @@
     col = lax.broadcasted_iota(jnp.int32, (qb, qb), 1)
     causal = col < row
     tri = (row >= col).astype(f32).astype(bf16)
-    bias_rows = []
-    for i in range(n_sp // 2):
+
+    def prepare(i):
         blocks = []
         v_blocks = []
         bias_i = []
@@ -333,38 +354,43 @@
             blocks.append(pack_r[b, 0:tok, :].astype(f32))
             vp = pack_r[b, tok : tok + half, :].astype(f32)
             v_blocks += [vp[:, :hd], vp[:, hd:]]
-            bias_i.append(pack_r[b, tok + half : tok + half + 16, :].astype(f32)[0:1])
+            bias_i.append(pack_r[b, tok + half : tok + half + 16, :].astype(f32)[0:8])
         both = jnp.concatenate(blocks, axis=0)
         q_i = both[:, :hd]
         k_i = both[:, hd:]
         q_i = q_i * lax.rsqrt(jnp.mean(q_i * q_i, axis=1, keepdims=True) + epsilon) * qg_ref[...]
         k_i = k_i * lax.rsqrt(jnp.mean(k_i * k_i, axis=1, keepdims=True) + epsilon) * kg_ref[...]
-        q_n = (q_i.astype(bf16).astype(f32) * hd**-0.5).astype(bf16)
+        qn_v[i] = (q_i.astype(bf16).astype(f32) * hd**-0.5).astype(bf16)
         kn_v[i] = k_i.astype(bf16)
         vn_v[i] = jnp.concatenate(v_blocks, axis=0).astype(bf16)
-        bias_rows.append(jnp.concatenate(bias_i, axis=1))
-        summed = jnp.zeros((qb, hd), f32)
-        carry = jnp.zeros((qb, 1), f32)
-        for j in range(i, -1, -1):
-            s = lax.dot_general(
-                q_n, kn_v[j], (((1,), (1,)), ((), ())), preferred_element_type=f32
-            )
-            s = s - bias_rows[j]
-            leave = jnp.maximum(s, 0.0) + jnp.log(1.0 + jnp.exp(-jnp.abs(s)))
-            if j == i:
-                leave = jnp.where(causal, leave, 0.0)
-            top = leave.astype(bf16)
-            low = (leave - top.astype(f32)).astype(bf16)
-            total = jnp.dot(top, tri, preferred_element_type=f32) + jnp.dot(
-                low, tri, preferred_element_type=f32
-            )
-            weight = jnp.exp(s - total - carry)
-            if j == i:
-                weight = jnp.where(causal, weight, 0.0)
-            carry = carry + total[:, 0:1]
-            summed = summed + jnp.dot(weight.astype(bf16), vn_v[j], preferred_element_type=f32)
-        for b in (2 * i, 2 * i + 1):
-            part = summed[(b - 2 * i) * tok : (b - 2 * i + 1) * tok]
+        bias_v[i] = jnp.concatenate(bias_i, axis=1)
+
+    def tile(i, j, state):
+        s = lax.dot_general(
+            qn_v[i], kn_v[j], (((1,), (1,)), ((), ())), preferred_element_type=f32
+        )
+        s = s - bias_v[j][0:1]
+        leave = jnp.maximum(s, 0.0) + jnp.log(1.0 + jnp.exp(-jnp.abs(s)))
+        if state is None:
+            leave = jnp.where(causal, leave, 0.0)
+        top = leave.astype(bf16)
+        low = (leave - top.astype(f32)).astype(bf16)
+        total = jnp.dot(top, tri, preferred_element_type=f32) + jnp.dot(
+            low, tri, preferred_element_type=f32
+        )
+        if state is None:
+            weight = jnp.where(causal, jnp.exp(s - total), 0.0)
+        else:
+            weight = jnp.exp(s - total - state[1])
+        part = jnp.dot(weight.astype(bf16), vn_v[j], preferred_element_type=f32)
+        if state is None:
+            return part, total[:, 0:1]
+        return state[0] + part, state[1] + total[:, 0:1]
+
+    def give_back(i, summed):
+        for r in range(2):
+            b = 2 * i + r
+            part = summed[r * tok : (r + 1) * tok]
             packed = jnp.concatenate([part[:half], part[half:]], axis=1).astype(bf16)
             att_s[b] = packed
 
@@ -375,6 +401,37 @@
             @pl.when(b == me)
             def _():
                 att_r[b] = packed
+
+    def triangle(half_id):
+        first = half_id * (quad // 2)
+        prepare(first)
+        prepare(first + 1)
+        state0 = tile(first, first, None)
+        state1 = tile(first + 1, first, tile(first + 1, first + 1, None))
+        for i, state in ((first, state0), (first + 1, state1)):
+            sum_v[i] = state[0]
+            carry_v[i] = jnp.broadcast_to(state[1], (qb, 128))
+
+    near_half = line // (quad // 2)
+    triangle(near_half)
+
+    @pl.when(near_half == 0)
+    def _():
+        for i in range(2):
+            give_back(i, sum_v[i])
+
+    triangle(1 - near_half)
+
+    @pl.when(near_half == 1)
+    def _():
+        for i in range(2):
+            give_back(i, sum_v[i])
+
+    for i in (2, 3):
+        state = (sum_v[i], carry_v[i][:, 0:1])
+        for j in (1, 0):
+            state = tile(i, j, state)
+        give_back(i, state[0])
 
     for h in range(n_sp):
 
@@ -417,12 +474,6 @@
     )
     for e in range(n_sp):
         disp_s[e] = spread[e * cap : (e + 1) * cap].astype(bf16)
-
-    quad = n_sp // 2
-    line = me // 2
-    side = me % 2
-    lines = [line, line + 1 - 2 * (line % 2), (line + 2) % quad, quad - 1 - line]
-    groups = [[2 * at + side for at in lines], [2 * at + 1 - side for at in lines]]
 
     def disp_copy(block, peer, slot):
         return send(
@@ -542,8 +593,8 @@
     second_pass(groups[1])
     step_over(0)
     expert_share(1, groups[1])
+    step_over(1)
     step_back(0)
-    step_over(1)
     step_back(1)
 
     for d in range(1, n_sp):
@@ -606,6 +657,14 @@
     anywhere = pl.BlockSpec(memory_space=pl.ANY)
     dma = pltpu.SemaphoreType.DMA
     scratch = [
+        pltpu.VMEM((tok, packed), bf16),
+        pltpu.VMEM((tok, packed), bf16),
+        pltpu.VMEM((tok, packed), bf16),
+        pltpu.VMEM((n_sp, tok), bf16),
+        pltpu.VMEM((pairs, 2 * tok, hd), bf16),
+        pltpu.VMEM((pairs, 8, 2 * tok), f32),
+        pltpu.VMEM((pairs, 2 * tok, hd), f32),
+        pltpu.VMEM((pairs, 2 * tok, 128), f32),
         pltpu.VMEM((tok, own), bf16),
         pltpu.VMEM((packed, model), bf16),
         pltpu.VMEM((model, hidden), bf16),
@@ -631,7 +690,7 @@
         pltpu.VMEM((2, quad, cap, own), bf16),
         pltpu.VMEM((n_sp, cap, own), bf16),
         pltpu.VMEM((n_sp, cap, own), bf16),
-        dma((5,)),
+        dma((9,)),
         dma((n_sp,)),
         dma((n_sp,)),
         dma((n_sp,)),
@@ -651,11 +710,11 @@
     return pl.pallas_call(
         functools.partial(fused_kernel, (n_sp, n_tp, tok, hd, cap, own)),
         out_shape=jax.ShapeDtypeStruct((tok, own), bf16),
-        in_specs=[vmem] * 9 + [anywhere] * 5,
+        in_specs=[anywhere] * 4 + [vmem] * 5 + [anywhere] * 5,
         out_specs=vmem,
         scratch_shapes=scratch,
         compiler_params=pltpu.CompilerParams(
-            collective_id=0, has_side_effects=True, vmem_limit_bytes=56 * 1024 * 1024
+            collective_id=0, has_side_effects=True, vmem_limit_bytes=63 * 1024 * 1024
         ),
     )(
         queries,

time: 61.2 us -> 60.6 us (level)
  no operation moved by 1% of the time
where the time goes in v3:
time: 60.6 us; the launch traced here: 60.5 us
  Pallas kernels  58.9 us (97%)
  local copies, waits for them, and re-layouts  1.57 us (3%)
    pallas_call x1, Pallas kernels, fused_device(): pl.pallas_call(functools.partial(fused_kernel, (n_sp, n_tp, tok, hd, cap,...  58.9 us
    unnamed x1, local copies, waits for them, and re-layouts  1.57 us

profile of v3, /device:TPU:0, one launch (start us, length us, event | category | flops | bytes accessed | tf_op | source)
XLA Modules:
  0.0 60.5 jit_solution(6573959570930069850)
XLA Ops:
  0.0 58.9 %shard_map.136 = bf16[128,512]{1,0:T(8,128)(2,1)} custom-call(bf16[128,512]{1,0:T(8,128)(2,1)} %q_hbm.1, bf16[128,512]{1,0:T(8,128)(2,1)} %k_hbm.1, bf16[128,512]{1,0:T(8,128)(2,1)} %v_hbm.1, bf16[8,128]{1,0:T(8,128)(2,1)} %bias_hbm.1, f32[1,64]{1,0:T(1,128)} %bitcast.8, f32[1,64]{1,0:T(1,128)} %bitcast.9, f32[1,2048]{1,0:T(1,128)} %bitcast.5, ...), custom_call_target="tpu_custom_call" | custom-call | tf_op jit(solution)/shard_map/pallas_call | solution.py:710
  58.9 1.6 %copy.16 = bf16[128,512]{1,0:T(8,128)(2,1)} copy(bf16[128,512]{1,0:T(8,128)(2,1)} %shard_map.136) | data formatting | bytes 262144
